TPU v7x, 32 devices: a whole 2x2x4 slice. The times are simulated.
32 devices in a mesh: grp: 2 (over y), sp: 4 (over z), tp: 4 (over x, core).
Axes of the slice: x: 2, y: 2, z: 4, core: 2. Of those that a mesh axis runs over, the one named last changes fastest.
Arguments:
- tokens: bfloat16 [24576, 2048], P(('grp', 'sp', 'tp')), parts along dimension 0, may hold values from -6 to 6
- gain_pre: float32 [2, 2048], replicated, may hold values from 0.1 to 1.9
- gain_post: float32 [2, 2048], replicated, may hold values from 0.1 to 1.9
- w_b: bfloat16 [2, 2048, 512], P(None, 'sp', 'tp'), may hold values from -0.125 to 0.125
- w_c: bfloat16 [2, 2048, 512], P(None, 'sp', 'tp'), may hold values from -0.125 to 0.125
- w_x: bfloat16 [2, 2048, 512], P(None, 'sp', 'tp'), may hold values from -0.125 to 0.125
- taps: float32 [2, 3, 512], replicated, may hold values from -3.5 to 3.5
- w_out: bfloat16 [2, 512, 2048], P(None, 'tp', 'sp'), may hold values from -0.25 to 0.25
Outputs:
- result: bfloat16 [24576, 2048], P(('grp', 'sp', 'tp')), parts along dimension 0
There are 2 independent parts, one for each index of `grp`. A program takes and returns all parts, laid end to end along the dimension named above; an argument that names none is the same for every part. Nothing has to cross between parts.
All inputs are finite; a program needn't handle non-finite values.
Results may differ from a plain program's by a relative error of at most 0.024.
Values may be sent and summed in bfloat16 or wider, within the bound.
A program may use at most 128 MiB of HBM per device.

v0:
```python
import jax
import jax.numpy as jnp
from jax import lax
from jax.sharding import PartitionSpec as P

epsilon = 1e-06


def for_sending(value):
    return jax.tree.map(lambda a: a.astype(jnp.bfloat16) if a.dtype == jnp.float32 else a, value)


def from_behind(block, axis, distance):
    devices = range(lax.axis_size(axis))
    route = [(i - distance, i) for i in devices if i - distance in devices]
    return lax.ppermute(block, axis, route)


def normed(activations, gain_row):
    values_f = activations.astype(jnp.float32)
    scale = lax.rsqrt(jnp.mean(values_f * values_f, axis=-1, keepdims=True) + epsilon)
    return values_f * scale * gain_row


def fold_into(hidden, pieces):
    return tuple(
        (
            jnp.dot(hidden, weight_piece, preferred_element_type=jnp.float32)
            for weight_piece in pieces
        )
    )


def convolve(extended, tap_rows):
    kernel_size = tap_rows.shape[0]
    row_total = extended.shape[0] - kernel_size + 1
    extended_f = extended.astype(jnp.float32)
    convolved = jnp.zeros((row_total, extended.shape[1]), jnp.float32)
    for offset in range(kernel_size):
        convolved = convolved + tap_rows[offset][None, :] * extended_f[offset : offset + row_total]
    return convolved


def layer_blocks(w_b, w_c, w_x, w_out, layer_index):
    return (
        lax.all_gather(w_b[layer_index], "tp", axis=1, tiled=True),
        lax.all_gather(w_c[layer_index], "tp", axis=1, tiled=True),
        lax.all_gather(w_x[layer_index], "tp", axis=1, tiled=True),
        lax.all_gather(w_out[layer_index], "tp", axis=0, tiled=True),
    )


def gated_inputs(stream, gain_row, weights):
    hidden = normed(stream, gain_row).astype(jnp.bfloat16)
    sums = fold_into(
        hidden,
        jax.tree.map(
            lambda part: lax.all_gather(part, "sp", axis=0, tiled=True), for_sending(weights)
        ),
    )
    gate_b, gate_c, values = (item.astype(jnp.bfloat16) for item in sums)
    product = (gate_c.astype(jnp.float32) * values.astype(jnp.float32)).astype(jnp.bfloat16)
    return (gate_b, product)


def mixed_output(residual, gate_b, extended, tap_rows, out_weight, gain_row):
    convolved = convolve(extended, tap_rows)
    weighted = (gate_b.astype(jnp.float32) * convolved).astype(jnp.bfloat16)
    branch = jnp.dot(
        weighted,
        lax.all_gather(out_weight, "sp", axis=1, tiled=True),
        preferred_element_type=jnp.float32,
    )
    return (residual.astype(jnp.float32) + normed(branch, gain_row)).astype(jnp.bfloat16)


def on_device(tokens, gain_pre, gain_post, w_b, w_c, w_x, taps, w_out):
    layer_total = gain_pre.shape[0]
    kernel_size = taps.shape[1]
    reach = kernel_size - 1
    stream = tokens
    before = from_behind(stream[-reach * layer_total :], ("sp", "tp"), 1)
    stream = jnp.concatenate([before, stream], axis=0)
    for layer_index in range(layer_total):
        blocks = layer_blocks(w_b, w_c, w_x, w_out, layer_index)
        gate_b, product = gated_inputs(stream, gain_pre[layer_index], blocks[:3])
        stream = mixed_output(
            stream[reach:],
            gate_b[reach:],
            product,
            taps[layer_index],
            blocks[3],
            gain_post[layer_index],
        )
    return stream


def solution(mesh):
    placed = (
        P(("grp", "sp", "tp"), None),
        P(),
        P(),
        P(None, "sp", "tp"),
        P(None, "sp", "tp"),
        P(None, "sp", "tp"),
        P(),
        P(None, "tp", "sp"),
    )
    return jax.shard_map(
        on_device,
        mesh=mesh,
        in_specs=placed,
        out_specs=P(("grp", "sp", "tp"), None),
        check_vma=False,
    )
```

profile of v0, /device:TPU:0, one launch (start us, length us, event | category | flops | bytes accessed | tf_op | source)
XLA Modules:
  0.0 399.7 jit_solution(17191552259109853232)
XLA Ops:
  6.5 0.0 copy-start.2
  6.5 0.0 all-gather.27.cloned.1.call-start
  6.5 1.0 fusion.68
  7.6 9.1 %all-gather.2 = bf16[1,512,512]{2,1,0:T(8,128)(2,1)} all-gather(bf16[1,512,128]{2,1,0:T(8,128)(2,1)S(1)} %get-tuple-element.9), channel_id=4, replica_groups=mesh['grp'=2,'sp'=4,'tp'=4] {'tp'}, dimensions={2}, use_global_device_ids=true | all-gather | bytes 655360 | tf_op jit(solution)/shard_map/all_gather | solution.py:47
  16.7 0.0 all-gather.27.cloned.1.call-update
  16.7 0.0 all-gather.25.cloned.1.call-start
  16.7 1.6 fusion.67
  18.4 7.7 %all-gather = bf16[1,512,512]{2,1,0:T(8,128)(2,1)} all-gather(bf16[1,512,128]{2,1,0:T(8,128)(2,1)S(1)} %get-tuple-element.8), channel_id=2, replica_groups=mesh['grp'=2,'sp'=4,'tp'=4] {'tp'}, dimensions={2}, use_global_device_ids=true | all-gather | bytes 655360 | tf_op jit(solution)/shard_map/all_gather | solution.py:46
  26.1 0.0 all-gather.25.cloned.1.call-update
  26.1 0.0 all-gather.29.cloned.1.call-start
  26.2 0.0 copy-done.2
  26.2 0.0 copy-start
  26.2 7.9 %all-gather.4 = bf16[1,512,512]{2,1,0:T(8,128)(2,1)} all-gather(bf16[1,512,128]{2,1,0:T(8,128)(2,1)S(1)} %get-tuple-element.11), channel_id=6, replica_groups=mesh['grp'=2,'sp'=4,'tp'=4] {'tp'}, dimensions={2}, use_global_device_ids=true | all-gather | bytes 655360 | tf_op jit(solution)/shard_map/all_gather | solution.py:48
  34.1 0.0 all-gather.29.cloned.1.call-update
  34.2 0.0 copy-start.3
  34.2 0.0 all-gather.31.cloned.1.call-start
  34.2 1.0 fusion.70
  35.2 7.7 %all-gather.6 = bf16[1,512,512]{2,1,0:T(8,128)(2,1)} all-gather(bf16[1,128,512]{2,1,0:T(8,128)(2,1)S(1)} %get-tuple-element.13), channel_id=8, replica_groups=mesh['grp'=2,'sp'=4,'tp'=4] {'tp'}, dimensions={1}, use_global_device_ids=true | all-gather | bytes 655360 | tf_op jit(solution)/shard_map/all_gather | solution.py:49
  42.9 0.0 all-gather.31.cloned.1.call-update
  43.0 0.0 all-gather.33.cloned.1.call-start
  43.0 8.9 %all-gather.8 = bf16[1,512,512]{2,1,0:T(8,128)(2,1)} all-gather(bf16[1,512,128]{2,1,0:T(8,128)(2,1)} %get-tuple-element.7), channel_id=10, replica_groups=mesh['grp'=2,'sp'=4,'tp'=4] {'tp'}, dimensions={2}, use_global_device_ids=true | all-gather | bytes 655360 | tf_op jit(solution)/shard_map/all_gather | solution.py:46
  51.9 0.0 all-gather.33.cloned.1.call-update
  52.0 0.0 all-gather.35.cloned.1.call-start
  52.0 7.8 %all-gather.10 = bf16[1,512,512]{2,1,0:T(8,128)(2,1)} all-gather(bf16[1,512,128]{2,1,0:T(8,128)(2,1)S(1)} %get-tuple-element.10), channel_id=12, replica_groups=mesh['grp'=2,'sp'=4,'tp'=4] {'tp'}, dimensions={2}, use_global_device_ids=true | all-gather | bytes 655360 | tf_op jit(solution)/shard_map/all_gather | solution.py:47
  59.8 0.0 all-gather.35.cloned.1.call-update
  59.8 0.0 all-gather.37.cloned.1.call-start
  59.8 7.8 %all-gather.12 = bf16[1,512,512]{2,1,0:T(8,128)(2,1)} all-gather(bf16[1,512,128]{2,1,0:T(8,128)(2,1)S(1)} %get-tuple-element.12), channel_id=14, replica_groups=mesh['grp'=2,'sp'=4,'tp'=4] {'tp'}, dimensions={2}, use_global_device_ids=true | all-gather | bytes 655360 | tf_op jit(solution)/shard_map/all_gather | solution.py:48
  67.6 0.0 all-gather.37.cloned.1.call-update
  67.6 0.0 all-gather.39.cloned.1.call-start
  67.7 0.0 copy-done
  67.7 2.3 collective-permute-start
  70.0 8.5 %all-gather.14 = bf16[1,512,512]{2,1,0:T(8,128)(2,1)} all-gather(bf16[1,128,512]{2,1,0:T(8,128)(2,1)S(1)} %get-tuple-element.14), channel_id=16, replica_groups=mesh['grp'=2,'sp'=4,'tp'=4] {'tp'}, dimensions={1}, use_global_device_ids=true | all-gather | bytes 655360 | tf_op jit(solution)/shard_map/all_gather | solution.py:49
  78.4 0.0 all-gather.39.cloned.1.call-update
  78.4 0.0 copy-done.3
  78.5 0.8 fusion.71
  79.3 0.8 fusion.73
  80.1 0.0 collective-permute-done
  80.1 1.2 fusion
  81.3 0.0 all-gather.27.cloned.1.call-done
  81.4 4.3 %fusion.31 = bf16[772,512]{1,0:T(8,128)(2,1)} fusion(bf16[1,2048,512]{2,1,0:T(8,128)(2,1)} %all-gather.27.cloned.1.call-done, f32[2048]{0:T(1024)S(1)} %bitcast.59, f32[772]{0:T(1024)S(1)} %add_rsqrt_fusion.3, bf16[768,2048]{1,0:T(8,128)(2,1)S(1)} %copy-done, bf16[4,2048]{1,0:T(4,128)(2,1)S(1)} %collective-permute-done), kind=kOutput, calls=%fused_computation.51 | convolution fusion | flops 1630464000 | bytes 6061072 | tf_op jit(solution)/shard_map/dot_general | solution.py:28
  85.7 23.8 %all-gather.25.cloned.1.call-done = bf16[1,2048,512]{2,1,0:T(8,128)(2,1)} async-done(((bf16[1,512,512]{2,1,0:T(8,128)(2,1)}), bf16[1,2048,512]{2,1,0:T(8,128)(2,1)}) %all-gather.25.cloned.1.call-update) | async-done | bytes 2097168 | tf_op jit(solution)/shard_map/all_gather | solution.py:58
  109.5 4.4 %fusion.21 = bf16[772,512]{1,0:T(8,128)(2,1)} fusion(bf16[1,2048,512]{2,1,0:T(8,128)(2,1)} %all-gather.25.cloned.1.call-done, f32[2048]{0:T(1024)S(1)} %bitcast.60, f32[772]{0:T(1024)S(1)} %add_rsqrt_fusion.3, bf16[768,2048]{1,0:T(8,128)(2,1)S(1)} %copy-done, bf16[4,2048]{1,0:T(4,128)(2,1)S(1)} %collective-permute-done), kind=kOutput, calls=%fused_computation.31 | convolution fusion | flops 1630068736 | bytes 6061072 | tf_op jit(solution)/shard_map/dot_general | solution.py:28
  113.8 41.7 %all-gather.29.cloned.1.call-done = bf16[1,2048,512]{2,1,0:T(8,128)(2,1)} async-done(((bf16[1,512,512]{2,1,0:T(8,128)(2,1)}), bf16[1,2048,512]{2,1,0:T(8,128)(2,1)}) %all-gather.29.cloned.1.call-update) | async-done | bytes 2097168 | tf_op jit(solution)/shard_map/all_gather | solution.py:58
  155.5 4.8 %fusion.50 = f32[772,512]{1,0:T(8,128)} fusion(bf16[1,2048,512]{2,1,0:T(8,128)(2,1)} %all-gather.29.cloned.1.call-done, bf16[772,512]{1,0:T(8,128)(2,1)} %fusion.31, f32[2048]{0:T(1024)S(1)} %bitcast.61, f32[772]{0:T(1024)S(1)} %add_rsqrt_fusion.3, bf16[768,2048]{1,0:T(8,128)(2,1)S(1)} %copy-done, bf16[4,2048]{1,0:T(4,128)(2,1)S(1)} %collective-permute-done), kind=kOutput, calls=%fused_computation.56 | convolution fusion | flops 1632440320 | bytes 7642128 | tf_op jit(solution)/shard_map/dot_general | solution.py:28
  160.3 41.1 %all-gather.31.cloned.1.call-done = bf16[1,512,2048]{2,1,0:T(8,128)(2,1)} async-done(((bf16[1,512,512]{2,1,0:T(8,128)(2,1)}), bf16[1,512,2048]{2,1,0:T(8,128)(2,1)}) %all-gather.31.cloned.1.call-update) | async-done | bytes 2097168 | tf_op jit(solution)/shard_map/all_gather | solution.py:71
  201.5 5.7 %multiply_reduce_fusion = (f32[770]{0:T(1024)S(1)}, f32[770,2048]{1,0:T(8,128)S(1)}) fusion(bf16[1,512,2048]{2,1,0:T(8,128)(2,1)} %all-gather.31.cloned.1.call-done, f32[772,512]{1,0:T(8,128)} %fusion.50, bf16[772,512]{1,0:T(8,128)(2,1)} %fusion.21, f32[512]{0:T(512)S(1)} %bitcast.65, f32[512]{0:T(512)S(1)} %bitcast.66, f32[512]{0:T(512)S(1)} %bitcast.67), kind=kOutput, calls=%fused_computation.11 | convolution fusion | flops 1621114112 | bytes 13976584 | tf_op jit(solution)/shard_map/dot_general | solution.py:69
  207.1 3.8 fusion.3
  211.0 36.4 %all-gather.33.cloned.1.call-done = bf16[1,2048,512]{2,1,0:T(8,128)(2,1)} async-done(((bf16[1,512,512]{2,1,0:T(8,128)(2,1)}), bf16[1,2048,512]{2,1,0:T(8,128)(2,1)}) %all-gather.33.cloned.1.call-update) | async-done | bytes 2097168 | tf_op jit(solution)/shard_map/all_gather | solution.py:58
  247.4 4.4 %fusion.13 = bf16[770,512]{1,0:T(8,128)(2,1)S(1)} fusion(bf16[1,2048,512]{2,1,0:T(8,128)(2,1)} %all-gather.33.cloned.1.call-done, bf16[770,2048]{1,0:T(8,128)(2,1)} %get-tuple-element.6, f32[2048]{0:T(1024)S(1)} %bitcast.56, f32[770]{0:T(1024)S(1)} %add_rsqrt_fusion.1), kind=kOutput, calls=%fused_computation.23 | convolution fusion | flops 1621114880 | bytes 6050824 | tf_op jit(solution)/shard_map/dot_general | solution.py:28
  251.8 41.5 %all-gather.35.cloned.1.call-done = bf16[1,2048,512]{2,1,0:T(8,128)(2,1)} async-done(((bf16[1,512,512]{2,1,0:T(8,128)(2,1)}), bf16[1,2048,512]{2,1,0:T(8,128)(2,1)}) %all-gather.35.cloned.1.call-update) | async-done | bytes 2097168 | tf_op jit(solution)/shard_map/all_gather | solution.py:58
  293.3 5.3 %fusion.37 = bf16[770,512]{1,0:T(8,128)(2,1)} fusion(bf16[1,2048,512]{2,1,0:T(8,128)(2,1)} %all-gather.35.cloned.1.call-done, bf16[770,2048]{1,0:T(8,128)(2,1)} %get-tuple-element.6, f32[2048]{0:T(1024)S(1)} %bitcast.57, f32[770]{0:T(1024)S(1)} %add_rsqrt_fusion.1), kind=kOutput, calls=%fused_computation.53 | convolution fusion | flops 1621509120 | bytes 6050824 | tf_op jit(solution)/shard_map/dot_general | solution.py:28
  298.6 40.8 %all-gather.37.cloned.1.call-done = bf16[1,2048,512]{2,1,0:T(8,128)(2,1)} async-done(((bf16[1,512,512]{2,1,0:T(8,128)(2,1)}), bf16[1,2048,512]{2,1,0:T(8,128)(2,1)}) %all-gather.37.cloned.1.call-update) | async-done | bytes 2097168 | tf_op jit(solution)/shard_map/all_gather | solution.py:58
  339.4 4.6 %fusion.45 = f32[770,512]{1,0:T(8,128)S(1)} fusion(bf16[1,2048,512]{2,1,0:T(8,128)(2,1)} %all-gather.37.cloned.1.call-done, bf16[770,512]{1,0:T(8,128)(2,1)} %fusion.37, bf16[770,2048]{1,0:T(8,128)(2,1)} %get-tuple-element.6, f32[2048]{0:T(1024)S(1)} %bitcast.58, f32[770]{0:T(1024)S(1)} %add_rsqrt_fusion.1), kind=kOutput, calls=%fused_computation.55 | convolution fusion | flops 1623480320 | bytes 7627784 | tf_op jit(solution)/shard_map/dot_general | solution.py:28
  343.9 41.5 %all-gather.39.cloned.1.call-done = bf16[1,512,2048]{2,1,0:T(8,128)(2,1)} async-done(((bf16[1,512,512]{2,1,0:T(8,128)(2,1)}), bf16[1,512,2048]{2,1,0:T(8,128)(2,1)}) %all-gather.39.cloned.1.call-update) | async-done | bytes 2097168 | tf_op jit(solution)/shard_map/all_gather | solution.py:71
  385.4 0.0 copy-start.1
  385.4 4.0 multiply_reduce_fusion.1
  389.4 0.0 copy-done.1
  389.4 3.5 add_convert_fusion.1
  (7 shorter events, 0.1 us)
Async XLA Ops:
  6.5 19.7 %copy-start.2 = (bf16[2,512,128]{2,1,0:T(8,128)(2,1)S(1)}, bf16[2,512,128]{2,1,0:T(8,128)(2,1)}, u32[]{:S(2)}) copy-start(bf16[2,512,128]{2,1,0:T(8,128)(2,1)} %param.13) | copy-start | bytes 786436
  6.5 74.8 %all-gather.27.cloned.1.call-start = ((), (), s32[]{:S(2)}) async-start(), calls=%async_computation.1 | async-start | bytes 2621440 | tf_op jit(solution)/shard_map/all_gather | solution.py:58
  16.7 92.8 %all-gather.25.cloned.1.call-start = ((), (), s32[]{:S(2)}) async-start(), calls=%async_computation | async-start | bytes 2621440 | tf_op jit(solution)/shard_map/all_gather | solution.py:58
  26.1 129.4 %all-gather.29.cloned.1.call-start = ((), (), s32[]{:S(2)}) async-start(), calls=%async_computation.2 | async-start | bytes 2621440 | tf_op jit(solution)/shard_map/all_gather | solution.py:58
  26.2 41.4 %copy-start = (bf16[768,2048]{1,0:T(8,128)(2,1)S(1)}, bf16[768,2048]{1,0:T(8,128)(2,1)}, u32[]{:S(2)}) copy-start(bf16[768,2048]{1,0:T(8,128)(2,1)} %param.8) | copy-start | bytes 9437188
  34.2 44.3 %copy-start.3 = (f32[2,2048]{1,0:T(2,128)S(1)}, f32[2,2048]{1,0:T(2,128)}, u32[]{:S(2)}) copy-start(f32[2,2048]{1,0:T(2,128)} %param.9) | copy-start | bytes 49156
  34.2 167.3 %all-gather.31.cloned.1.call-start = ((), (), s32[]{:S(2)}) async-start(), calls=%async_computation.3 | async-start | bytes 2621440 | tf_op jit(solution)/shard_map/all_gather | solution.py:71
  43.0 204.4 %all-gather.33.cloned.1.call-start = ((), (), s32[]{:S(2)}) async-start(), calls=%async_computation.4 | async-start | bytes 2621440 | tf_op jit(solution)/shard_map/all_gather | solution.py:58
  52.0 241.3 %all-gather.35.cloned.1.call-start = ((), (), s32[]{:S(2)}) async-start(), calls=%async_computation.5 | async-start | bytes 2621440 | tf_op jit(solution)/shard_map/all_gather | solution.py:58
  59.8 279.6 %all-gather.37.cloned.1.call-start = ((), (), s32[]{:S(2)}) async-start(), calls=%async_computation.6 | async-start | bytes 2621440 | tf_op jit(solution)/shard_map/all_gather | solution.py:58
  67.6 317.8 %all-gather.39.cloned.1.call-start = ((), (), s32[]{:S(2)}) async-start(), calls=%async_computation.7 | async-start | bytes 2621440 | tf_op jit(solution)/shard_map/all_gather | solution.py:71
  67.7 12.4 %collective-permute-start = (bf16[4,2048]{1,0:T(4,128)(2,1)S(1)}, bf16[4,2048]{1,0:T(4,128)(2,1)S(1)}, u32[]{:S(2)}, u32[]{:S(2)}) collective-permute-start(bf16[4,2048]{1,0:T(4,128)(2,1)S(1)} %slice.101), channel_id=1, source_target_pairs={{0,1},{1,2},{2,3},{3,4},{4,5},{5,6},{6,7},{7,8},{8,9},{9,10},{10,1... | collective-permute-start | bytes 49160 | tf_op jit(solution)/shard_map/ppermute | solution.py:16
  385.4 4.0 %copy-start.1 = (bf16[770,2048]{1,0:T(8,128)(2,1)S(1)}, bf16[770,2048]{1,0:T(8,128)(2,1)}, u32[]{:S(2)}) copy-start(bf16[770,2048]{1,0:T(8,128)(2,1)} %get-tuple-element.6) | copy-start | bytes 9461764
Sparse Core Ops, SparseCore 0:
  16.8 46.5 all-gather.26
  65.0 44.4 all-gather.24
  111.0 44.4 all-gather.28
  157.0 44.4 all-gather.30
  202.9 44.4 all-gather.32
  248.8 44.4 all-gather.34
  294.9 44.4 all-gather.36
  340.9 44.4 all-gather.38
where the time goes:
time: 400 us
  waiting for transfers between devices  267 us (67%)
  blocking collectives  65.3 us (16%)
  matrix products  37.5 us (9%)
  between operations  13.6 us (3%)
  other arithmetic  8.54 us (2%)
  local copies, waits for them, and re-layouts  5.33 us (1%)
    all_gather x6, waiting for transfers between devices, gated_inputs(): lax.all_gather(part, 'sp', axis=0, tiled=True)  184 us
    all_gather x2, waiting for transfers between devices, mixed_output(): lax.all_gather(out_weight, 'sp', axis=1, tiled=True)  82.6 us
    dot_general x6, matrix products, fold_into(): jnp.dot(hidden, weight_piece, preferred_element_type=jnp.float32)  27.8 us
    all_gather x2, blocking collectives, layer_blocks(): lax.all_gather(w_c[layer_index], 'tp', axis=1, tiled=True)  16.8 us
    all_gather x2, blocking collectives, layer_blocks(): lax.all_gather(w_b[layer_index], 'tp', axis=1, tiled=True)  16.7 us
    all_gather x2, blocking collectives, layer_blocks(): lax.all_gather(w_out[layer_index], 'tp', axis=0, tiled=True)  16.2 us
    all_gather x2, blocking collectives, layer_blocks(): lax.all_gather(w_x[layer_index], 'tp', axis=1, tiled=True)  15.6 us
    dot_general x2, matrix products, mixed_output(): jnp.dot(weighted, lax.all_gather(out_weight, 'sp', axis=1, tiled=True), p...  9.67 us
  transfers between devices with their start and end apart: 9, of which 7 were waited for; matrix products, arithmetic and copies ran while one was open for 11% of the time, Pallas kernels for 0%

commit v1 on v0

--- a/solution.py
+++ b/solution.py
@@ -1,9 +1,14 @@
+import functools
+
 import jax
 import jax.numpy as jnp
 from jax import lax
+from jax.experimental import pallas as pl
+from jax.experimental.pallas import tpu as pltpu
 from jax.sharding import PartitionSpec as P
 
 epsilon = 1e-06
+MESH = pl.DeviceIdType.MESH
 
 
 def for_sending(value):
@@ -95,6 +100,422 @@
     return stream
 
 
+def unit_views(units, win, wout):
+    def view(unit, s, t, start, count, rows, cols):
+        layer, kind = units[unit]
+        if kind == 0:
+            return win.at[
+                layer,
+                :,
+                pl.ds(pl.multiple_of(s * rows + start, 16), count),
+                pl.ds(pl.multiple_of(t * cols, 128), cols),
+            ]
+        return wout.at[
+            layer,
+            pl.ds(pl.multiple_of(t * cols + start, 16), count),
+            pl.ds(pl.multiple_of(s * rows, 128), rows),
+        ]
+
+    return view
+
+
+def up_to(fraction_num, fraction_den, total):
+    return -(-(total * fraction_num // fraction_den) // 16) * 16
+
+
+def mixer_kernel(
+    sp, tp, halo, tok, gain_pre, gain_post, w_b, w_c, w_x, taps, w_out, out,
+    win, wout, xs, hid, gated, prod,
+    load_sem, halo_sem, z_send, z_recv, x_send, x_recv, y1_send, y1_recv,
+    y2_send, y2_recv, d_send, d_recv, out_sem,
+):
+    layers = w_b.shape[0]
+    rows, cols = w_b.shape[1], w_b.shape[2]
+    own_tokens = tok.shape[0]
+    total_rows = own_tokens + halo
+    channels = win.shape[3]
+    y = lax.axis_index("grp")
+    z = lax.axis_index("sp")
+    t = lax.axis_index("tp")
+    core = lax.rem(t, 2)
+    x = t // 2
+    t_x = (1 - x) * 2 + core
+    t_core = x * 2 + 1 - core
+    t_both = (1 - x) * 2 + 1 - core
+    units = [(layer, kind) for layer in range(layers) for kind in (0, 1)]
+    view = unit_views(units, win, wout)
+
+    def sizes(unit):
+        n = rows if units[unit][1] == 0 else cols
+        return n, up_to(3, 4, n), up_to(19, 32, n)
+
+    def block(unit, s, tt, start, count):
+        return view(unit, s, tt, start, count, rows, cols)
+
+    def send(ref, send_sem, recv_sem, where):
+        return pltpu.make_async_remote_copy(
+            src_ref=ref, dst_ref=ref, send_sem=send_sem, recv_sem=recv_sem,
+            device_id=where, device_id_type=MESH,
+        )
+
+    def z_copy(u, s, up):
+        n, nz, _ = sizes(u)
+        return send(
+            block(u, s, t, y * (n - nz), nz), z_send.at[u, s, up], z_recv.at[u, s],
+            {"sp": z + (1 if up else -1)},
+        )
+
+    def x_copy(u, s, tt):
+        n, _, nx = sizes(u)
+        return send(
+            block(u, s, tt, y * (n - nx), nx), x_send.at[u, s], x_recv.at[u, s], {"tp": t_x}
+        )
+
+    def y1_copy(u, s, yy):
+        n, nz, _ = sizes(u)
+        return send(
+            block(u, s, t, yy * nz, n - nz), y1_send.at[u, s], y1_recv.at[u, s], {"grp": 1 - y}
+        )
+
+    def y2_copy(u, s, yy):
+        n, _, nx = sizes(u)
+        return send(
+            block(u, s, t_x, yy * nx, n - nx), y2_send.at[u, s], y2_recv.at[u, s], {"grp": 1 - y}
+        )
+
+    def d_copy(u, s, other, tt):
+        n, _, _ = sizes(u)
+        return send(
+            block(u, s, tt, 0, n), d_send.at[u, s, other], d_recv.at[u, s, other], {"tp": t_core}
+        )
+
+    def at_distance(j, act):
+        if j == 0:
+            act(z, None)
+            return
+
+        @pl.when(z + j < sp)
+        def _():
+            act(z + j, 0)
+
+        @pl.when(z >= j)
+        def _():
+            act(z - j, 1)
+
+    def own(u):
+        @pl.when(z + 1 < sp)
+        def _():
+            z_copy(u, z, 1).start()
+
+        @pl.when(z >= 1)
+        def _():
+            z_copy(u, z, 0).start()
+
+        x_copy(u, z, t).start()
+        d_copy(u, z, 0, t).start()
+
+    def wave_z(u, j):
+        def act(s, up):
+            z_copy(u, s, up).wait_recv()
+            if up:
+                @pl.when(z + 1 < sp)
+                def _():
+                    z_copy(u, s, 1).start()
+            else:
+                @pl.when(z >= 1)
+                def _():
+                    z_copy(u, s, 0).start()
+            x_copy(u, s, t).start()
+            y1_copy(u, s, y).start()
+
+        at_distance(j, act)
+
+    def wave_x(u, j):
+        def act(s, _):
+            x_copy(u, s, t_x).wait_recv()
+            y2_copy(u, s, y).start()
+
+        at_distance(j, act)
+
+    def wave_y(u, j):
+        def act(s, _):
+            if j > 0:
+                y1_copy(u, s, 1 - y).wait_recv()
+                d_copy(u, s, 0, t).start()
+            y2_copy(u, s, 1 - y).wait_recv()
+            d_copy(u, s, 1, t_x).start()
+
+        at_distance(j, act)
+
+    def arrived(u):
+        for j in range(sp):
+            def act(s, _):
+                d_copy(u, s, 0, t_core).wait_recv()
+                d_copy(u, s, 1, t_both).wait_recv()
+
+            at_distance(j, act)
+
+    def sent(u):
+        for j in range(sp):
+            def act(s, up):
+                if j == 0:
+                    @pl.when(z + 1 < sp)
+                    def _():
+                        z_copy(u, s, 1).wait_send()
+
+                    @pl.when(z >= 1)
+                    def _():
+                        z_copy(u, s, 0).wait_send()
+                else:
+                    if up:
+                        @pl.when(z + 1 < sp)
+                        def _():
+                            z_copy(u, s, 1).wait_send()
+                    else:
+                        @pl.when(z >= 1)
+                        def _():
+                            z_copy(u, s, 0).wait_send()
+                    y1_copy(u, s, y).wait_send()
+                x_copy(u, s, t).wait_send()
+                y2_copy(u, s, y).wait_send()
+                d_copy(u, s, 0, t).wait_send()
+                d_copy(u, s, 1, t_x).wait_send()
+
+            at_distance(j, act)
+
+    def scaled(value_f, gain_row):
+        scale = lax.rsqrt(jnp.mean(value_f * value_f, axis=-1, keepdims=True) + epsilon)
+        return value_f * scale * gain_row
+
+    def project_in(layer, part, width):
+        cut = pl.ds(part * width, width)
+        hidden = hid[...]
+
+        def through(which):
+            return jnp.dot(
+                hidden, win[layer, which, :, cut], preferred_element_type=jnp.float32
+            ).astype(jnp.bfloat16).astype(jnp.float32)
+
+        product = (through(1) * through(2)).astype(jnp.bfloat16).astype(jnp.float32)
+        reach = taps.shape[1] - 1
+        prod[pl.ds(8, total_rows), :] = product
+        conv = taps[layer, reach, cut][None, :] * product
+        for k in range(reach):
+            conv = conv + taps[layer, k, cut][None, :] * prod[pl.ds(8 - reach + k, total_rows), :]
+        gated[:, cut] = (through(0) * conv).astype(jnp.bfloat16)
+
+    def project_out(layer, start, count):
+        where = pl.ds(start, count)
+        branch = jnp.dot(gated[where, :], wout[layer], preferred_element_type=jnp.float32)
+        added = xs[where, :].astype(jnp.float32) + scaled(branch, gain_post[layer][None, :])
+        stream = added.astype(jnp.bfloat16)
+        xs[where, :] = stream
+        if layer + 1 < layers:
+            hid[where, :] = scaled(
+                stream.astype(jnp.float32), gain_pre[layer + 1][None, :]
+            ).astype(jnp.bfloat16)
+
+    loads = []
+    for layer in range(layers):
+        for which, ref in enumerate((w_b, w_c, w_x)):
+            loads.append(
+                pltpu.make_async_copy(
+                    ref.at[layer],
+                    win.at[
+                        layer,
+                        which,
+                        pl.ds(pl.multiple_of(z * rows, 16), rows),
+                        pl.ds(pl.multiple_of(t * cols, 128), cols),
+                    ],
+                    load_sem.at[4 * layer + which],
+                )
+            )
+        loads.append(
+            pltpu.make_async_copy(
+                w_out.at[layer],
+                wout.at[
+                    layer,
+                    pl.ds(pl.multiple_of(t * cols, 16), cols),
+                    pl.ds(pl.multiple_of(z * rows, 128), rows),
+                ],
+                load_sem.at[4 * layer + 3],
+            )
+        )
+    tokens_in = pltpu.make_async_copy(
+        tok, xs.at[pl.ds(halo, own_tokens)], load_sem.at[4 * layers]
+    )
+    for load in loads:
+        load.start()
+    tokens_in.start()
+
+    place = z * tp + t
+    after = lax.rem(place + 1, sp * tp)
+
+    def halo_copy():
+        return pltpu.make_async_remote_copy(
+            src_ref=tok.at[pl.ds(own_tokens - halo, halo)],
+            dst_ref=xs.at[pl.ds(0, halo)],
+            send_sem=halo_sem.at[0],
+            recv_sem=halo_sem.at[1],
+            device_id={"sp": after // tp, "tp": lax.rem(after, tp)},
+            device_id_type=MESH,
+        )
+
+    for load in loads:
+        load.wait()
+    own(0)
+
+    @pl.when(place + 1 < sp * tp)
+    def _():
+        halo_copy().start()
+
+    own(1)
+    prod[pl.ds(0, 8), :] = jnp.zeros((8, prod.shape[1]), jnp.float32)
+
+    @pl.when(place == 0)
+    def _():
+        xs[pl.ds(0, halo), :] = jnp.zeros((halo, xs.shape[1]), jnp.bfloat16)
+
+    tokens_in.wait()
+
+    def first_norm(start, count):
+        where = pl.ds(start, count)
+        hid[where, :] = scaled(xs[where, :].astype(jnp.float32), gain_pre[0][None, :]).astype(
+            jnp.bfloat16
+        )
+
+    piece = own_tokens // 3
+    for i in range(3):
+        first_norm(halo + i * piece, piece)
+
+    @pl.when(place > 0)
+    def _():
+        halo_copy().wait_recv()
+
+    first_norm(0, halo)
+
+    steps = sp - 1
+    width = prod.shape[1]
+    parts = channels // width
+    work = {}
+
+    def result_copy(i):
+        return pltpu.make_async_copy(
+            xs.at[pl.ds(halo + i * piece, piece)],
+            out.at[pl.ds(i * piece, piece)],
+            out_sem.at[i],
+        )
+
+    def last_rows(layer, i):
+        project_out(layer, halo + i * piece, piece)
+        if layer == layers - 1:
+            result_copy(i).start()
+
+    last_step = steps * len(units) + 2
+    for u, (layer, kind) in enumerate(units):
+        ready = min(steps * u + steps + 2, last_step)
+        todo = [functools.partial(arrived, u)]
+        if kind == 0:
+            todo += [functools.partial(project_in, layer, p, width) for p in range(parts)]
+        else:
+            todo += [functools.partial(last_rows, layer, i) for i in range(3)]
+            if layer + 1 < layers:
+                todo.append(functools.partial(project_out, layer, 0, halo))
+        for k, task in enumerate(todo):
+            work.setdefault(min(ready + max(k - 1, 0), last_step), []).append(task)
+
+    for g in range(1, last_step + 1):
+        u, j = (g - 1) // steps, (g - 1) % steps + 1
+        if u < len(units):
+            if j == 1 and 1 <= u < len(units) - 1:
+                own(u + 1)
+            wave_z(u, j)
+        for late, wave in ((1, wave_x), (2, wave_y)):
+            v, k = (g - 1 - late) // steps, (g - 1 - late) % steps + 1
+            if k == 1 and 0 <= v < len(units):
+                wave(v, 0)
+            if 0 <= v < len(units):
+                wave(v, k)
+        for task in work.get(g, []):
+            task()
+
+    for u in range(len(units)):
+        sent(u)
+
+    @pl.when(place + 1 < sp * tp)
+    def _():
+        halo_copy().wait_send()
+
+    for i in range(3):
+        result_copy(i).wait()
+
+
+def in_one_kernel(sp, tp, tokens, gain_pre, gain_post, w_b, w_c, w_x, taps, w_out):
+    layers, rows, cols = w_b.shape
+    own_tokens, width = tokens.shape
+    channels = cols * tp
+    halo = 16
+    units = 2 * layers
+    any_space = pl.BlockSpec(memory_space=pl.ANY)
+    vmem = pl.BlockSpec(memory_space=pltpu.VMEM)
+    dma = pltpu.SemaphoreType.DMA
+    part = min(256, channels)
+    return pl.pallas_call(
+        functools.partial(mixer_kernel, sp, tp, halo),
+        out_shape=jax.ShapeDtypeStruct(tokens.shape, tokens.dtype),
+        in_specs=[any_space, vmem, vmem, any_space, any_space, any_space, vmem, any_space],
+        out_specs=any_space,
+        scratch_shapes=[
+            pltpu.VMEM((layers, 3, rows * sp, channels), jnp.bfloat16),
+            pltpu.VMEM((layers, channels, rows * sp), jnp.bfloat16),
+            pltpu.VMEM((own_tokens + halo, width), jnp.bfloat16),
+            pltpu.VMEM((own_tokens + halo, width), jnp.bfloat16),
+            pltpu.VMEM((own_tokens + halo, channels), jnp.bfloat16),
+            pltpu.VMEM((own_tokens + halo + 8, part), jnp.float32),
+            dma((4 * layers + 1,)),
+            dma((2,)),
+            dma((units, sp, 2)),
+            dma((units, sp)),
+            dma((units, sp)),
+            dma((units, sp)),
+            dma((units, sp)),
+            dma((units, sp)),
+            dma((units, sp)),
+            dma((units, sp)),
+            dma((units, sp, 2)),
+            dma((units, sp, 2)),
+            dma((3,)),
+        ],
+        compiler_params=pltpu.CompilerParams(
+            has_side_effects=True, vmem_limit_bytes=60 * 1024 * 1024
+        ),
+    )(tokens, gain_pre, gain_post, w_b, w_c, w_x, taps, w_out)
+
+
+def kernel_fits(sizes, tokens, w_b, w_out, taps):
+    rows, cols = w_b.shape[1], w_b.shape[2]
+    layers = w_b.shape[0]
+    held = (4 * layers * rows * sizes["sp"] * cols * sizes["tp"]) * 2
+    held += 3 * tokens.shape[0] * tokens.shape[1] * 2
+    return (
+        sizes["grp"] == 2
+        and sizes["tp"] == 4
+        and rows % 128 == 0
+        and cols % 128 == 0
+        and tokens.shape[0] % 48 == 0
+        and (taps.shape[1] - 1) * layers <= 16
+        and taps.shape[1] <= 9
+        and held < 40 * 2**20
+    )
+
+
+def any_mesh(sizes, *arguments):
+    tokens, w_b, taps, w_out = arguments[0], arguments[3], arguments[6], arguments[7]
+    if kernel_fits(sizes, tokens, w_b, w_out, taps):
+        return in_one_kernel(sizes["sp"], sizes["tp"], *arguments)
+    return on_device(*arguments)
+
+
 def solution(mesh):
     placed = (
         P(("grp", "sp", "tp"), None),
@@ -107,7 +528,7 @@
         P(None, "tp", "sp"),
     )
     return jax.shard_map(
-        on_device,
+        functools.partial(any_mesh, dict(mesh.shape)),
         mesh=mesh,
         in_specs=placed,
         out_specs=P(("grp", "sp", "tp"), None),

time: 400 us -> 110 us (0.28)
  waiting for transfers between devices: 267 us -> 0 us
  Pallas kernels: 0 us -> 104 us
  blocking collectives: 65.3 us -> 0 us
  matrix products: 37.5 us -> 0 us
  between operations: 13.6 us -> 0.01 us
  other arithmetic: 8.54 us -> 0 us
    all_gather x8 -> x0, waiting for transfers between devices: 267 us -> none  [the longest x6 184 us: gated_inputs(): lax.all_gather(part, 'sp', axis=0, tiled=True)]
    pallas_call x0 -> x1, Pallas kernels: none -> 104 us  [in_one_kernel(): pl.pallas_call(functools.partial(mixer_kernel, sp, tp, halo), out_shape=j...]
    all_gather x8 -> x0, blocking collectives: 65.3 us -> none  [the longest x2 16.8 us: layer_blocks(): lax.all_gather(w_c[layer_index], 'tp', axis=1, tiled=True)]
    dot_general x8 -> x0, matrix products: 37.5 us -> none  [the longest x6 27.8 us: fold_into(): jnp.dot(hidden, weight_piece, preferred_element_type=jnp.float32)]
    slice x8 -> x0, local copies, waits for them, and re-layouts: 5.31 us -> none  [the longest x1 1.64 us: layer_blocks(): w_b[layer_index]]
    unnamed x8 -> x2, local copies, waits for them, and re-layouts: 0.02 us -> 5.28 us
    reduce_sum x2 -> x0, other arithmetic: 5.06 us -> none  [normed(): jnp.mean(values_f * values_f, axis=-1, keepdims=True) + epsilon]
  transfers between devices with their start and end apart: 9 -> 0, of which waited for: 7 -> 0; matrix products, arithmetic and copies ran while one was open for 11% -> 0% of each run, Pallas kernels for 0% -> 0%
where the time goes in v1:
time: 110 us; the launch traced here: 109 us
  Pallas kernels  104 us (95%)
  local copies, waits for them, and re-layouts  5.28 us (5%)
    pallas_call x1, Pallas kernels, in_one_kernel(): pl.pallas_call(functools.partial(mixer_kernel, sp, tp, halo), out_shape=j...  104 us
    unnamed x2, local copies, waits for them, and re-layouts  5.28 us

profile of v1, /device:TPU:0, one launch (start us, length us, event | category | flops | bytes accessed | tf_op | source)
XLA Modules:
  0.0 109.5 jit_solution(6118922510860263689)
XLA Ops:
  0.0 1.3 %copy.9.taps = f32[2,3,512]{2,1,0:T(4,128)} copy(f32[2,3,512]{2,0,1:T(2,128)} %param.14) | data formatting | bytes 24576 | tf_op args[6]
  1.3 104.2 %shard_map.82 = bf16[768,2048]{1,0:T(8,128)(2,1)} custom-call(bf16[768,2048]{1,0:T(8,128)(2,1)} %tok.1, f32[2,2048]{1,0:T(2,128)} %gain_pre.1, f32[2,2048]{1,0:T(2,128)} %gain_post.1, bf16[2,512,128]{2,1,0:T(8,128)(2,1)} %w_b.1, bf16[2,512,128]{2,1,0:T(8,128)(2,1)} %w_c.1, bf16[2,512,128]{2,1,0:T(8,128)(2,1)} %w_x.1, f32[2,3,512]{2,1,0:T(4,128)} %copy.9.taps, ...), custom_call_target="tpu_custom_call" | custom-call | tf_op jit(solution)/shard_map/pallas_call | solution.py:463
  105.5 4.0 %copy.11 = bf16[768,2048]{1,0:T(8,128)(2,1)} copy(bf16[768,2048]{1,0:T(8,128)(2,1)} %shard_map.82) | data formatting | bytes 6291456

commit v2 on v1

--- a/solution.py
+++ b/solution.py
@@ -103,10 +103,10 @@
 def unit_views(units, win, wout):
     def view(unit, s, t, start, count, rows, cols):
         layer, kind = units[unit]
-        if kind == 0:
+        if kind < 3:
             return win.at[
                 layer,
-                :,
+                kind,
                 pl.ds(pl.multiple_of(s * rows + start, 16), count),
                 pl.ds(pl.multiple_of(t * cols, 128), cols),
             ]
@@ -127,7 +127,7 @@
     sp, tp, halo, tok, gain_pre, gain_post, w_b, w_c, w_x, taps, w_out, out,
     win, wout, xs, hid, gated, prod,
     load_sem, halo_sem, z_send, z_recv, x_send, x_recv, y1_send, y1_recv,
-    y2_send, y2_recv, d_send, d_recv, out_sem,
+    y2_send, y2_recv, d_send, d_recv,
 ):
     layers = w_b.shape[0]
     rows, cols = w_b.shape[1], w_b.shape[2]
@@ -142,11 +142,11 @@
     t_x = (1 - x) * 2 + core
     t_core = x * 2 + 1 - core
     t_both = (1 - x) * 2 + 1 - core
-    units = [(layer, kind) for layer in range(layers) for kind in (0, 1)]
+    units = [(layer, kind) for layer in range(layers) for kind in range(4)]
     view = unit_views(units, win, wout)
 
     def sizes(unit):
-        n = rows if units[unit][1] == 0 else cols
+        n = rows if units[unit][1] < 3 else cols
         return n, up_to(3, 4, n), up_to(19, 32, n)
 
     def block(unit, s, tt, start, count):
@@ -297,11 +297,11 @@
             ).astype(jnp.bfloat16).astype(jnp.float32)
 
         product = (through(1) * through(2)).astype(jnp.bfloat16).astype(jnp.float32)
-        reach = taps.shape[1] - 1
+        reach = taps.shape[0] - 1
         prod[pl.ds(8, total_rows), :] = product
-        conv = taps[layer, reach, cut][None, :] * product
+        conv = taps[reach, layer, cut][None, :] * product
         for k in range(reach):
-            conv = conv + taps[layer, k, cut][None, :] * prod[pl.ds(8 - reach + k, total_rows), :]
+            conv = conv + taps[k, layer, cut][None, :] * prod[pl.ds(8 - reach + k, total_rows), :]
         gated[:, cut] = (through(0) * conv).astype(jnp.bfloat16)
 
     def project_out(layer, start, count):
@@ -309,11 +309,38 @@
         branch = jnp.dot(gated[where, :], wout[layer], preferred_element_type=jnp.float32)
         added = xs[where, :].astype(jnp.float32) + scaled(branch, gain_post[layer][None, :])
         stream = added.astype(jnp.bfloat16)
-        xs[where, :] = stream
         if layer + 1 < layers:
+            xs[where, :] = stream
             hid[where, :] = scaled(
                 stream.astype(jnp.float32), gain_pre[layer + 1][None, :]
             ).astype(jnp.bfloat16)
+        else:
+            out[pl.ds(start - halo, count), :] = stream
+
+    place = z * tp + t
+    ready = pltpu.get_barrier_semaphore()
+
+    def greet(where):
+        pl.semaphore_signal(ready, inc=1, device_id=where, device_id_type=MESH)
+
+    for where in ({"tp": t_x}, {"tp": t_core}, {"grp": 1 - y}):
+        greet(where)
+
+    @pl.when(z + 1 < sp)
+    def _():
+        greet({"sp": z + 1})
+
+    @pl.when(z >= 1)
+    def _():
+        greet({"sp": z - 1})
+
+    odd = lax.rem(t, 2)
+    partner = place + 2 * odd - 1
+    outside = jnp.logical_and(partner >= 0, partner < sp * tp)
+
+    @pl.when(outside)
+    def _():
+        greet({"sp": partner // tp, "tp": lax.rem(partner, tp)})
 
     loads = []
     for layer in range(layers):
@@ -348,7 +375,6 @@
         load.start()
     tokens_in.start()
 
-    place = z * tp + t
     after = lax.rem(place + 1, sp * tp)
 
     def halo_copy():
@@ -361,6 +387,13 @@
             device_id_type=MESH,
         )
 
+    greeted = (
+        3
+        + jnp.where(z + 1 < sp, 1, 0)
+        + jnp.where(z >= 1, 1, 0)
+        + jnp.where(outside, 1, 0)
+    )
+    pl.semaphore_wait(ready, greeted)
     for load in loads:
         load.wait()
     own(0)
@@ -399,25 +432,17 @@
     parts = channels // width
     work = {}
 
-    def result_copy(i):
-        return pltpu.make_async_copy(
-            xs.at[pl.ds(halo + i * piece, piece)],
-            out.at[pl.ds(i * piece, piece)],
-            out_sem.at[i],
-        )
-
     def last_rows(layer, i):
         project_out(layer, halo + i * piece, piece)
-        if layer == layers - 1:
-            result_copy(i).start()
-
-    last_step = steps * len(units) + 2
+
+    late_x, late_y = 2, 4
+    last_step = steps * len(units) + late_y
     for u, (layer, kind) in enumerate(units):
-        ready = min(steps * u + steps + 2, last_step)
+        ready = min(steps * u + steps + late_y, last_step)
         todo = [functools.partial(arrived, u)]
-        if kind == 0:
+        if kind == 2:
             todo += [functools.partial(project_in, layer, p, width) for p in range(parts)]
-        else:
+        if kind == 3:
             todo += [functools.partial(last_rows, layer, i) for i in range(3)]
             if layer + 1 < layers:
                 todo.append(functools.partial(project_out, layer, 0, halo))
@@ -430,7 +455,7 @@
             if j == 1 and 1 <= u < len(units) - 1:
                 own(u + 1)
             wave_z(u, j)
-        for late, wave in ((1, wave_x), (2, wave_y)):
+        for late, wave in ((late_x, wave_x), (late_y, wave_y)):
             v, k = (g - 1 - late) // steps, (g - 1 - late) % steps + 1
             if k == 1 and 0 <= v < len(units):
                 wave(v, 0)
@@ -446,25 +471,22 @@
     def _():
         halo_copy().wait_send()
 
-    for i in range(3):
-        result_copy(i).wait()
-
 
 def in_one_kernel(sp, tp, tokens, gain_pre, gain_post, w_b, w_c, w_x, taps, w_out):
     layers, rows, cols = w_b.shape
     own_tokens, width = tokens.shape
     channels = cols * tp
     halo = 16
-    units = 2 * layers
+    units = 4 * layers
     any_space = pl.BlockSpec(memory_space=pl.ANY)
     vmem = pl.BlockSpec(memory_space=pltpu.VMEM)
     dma = pltpu.SemaphoreType.DMA
     part = min(256, channels)
     return pl.pallas_call(
         functools.partial(mixer_kernel, sp, tp, halo),
-        out_shape=jax.ShapeDtypeStruct(tokens.shape, tokens.dtype),
+        out_shape=pltpu.VMEM(tokens.shape, tokens.dtype),
         in_specs=[any_space, vmem, vmem, any_space, any_space, any_space, vmem, any_space],
-        out_specs=any_space,
+        out_specs=vmem,
         scratch_shapes=[
             pltpu.VMEM((layers, 3, rows * sp, channels), jnp.bfloat16),
             pltpu.VMEM((layers, channels, rows * sp), jnp.bfloat16),
@@ -484,12 +506,11 @@
             dma((units, sp)),
             dma((units, sp, 2)),
             dma((units, sp, 2)),
-            dma((3,)),
         ],
         compiler_params=pltpu.CompilerParams(
-            has_side_effects=True, vmem_limit_bytes=60 * 1024 * 1024
+            has_side_effects=True, collective_id=0, vmem_limit_bytes=56000 * 1024
         ),
-    )(tokens, gain_pre, gain_post, w_b, w_c, w_x, taps, w_out)
+    )(tokens, gain_pre, gain_post, w_b, w_c, w_x, jnp.swapaxes(taps, 0, 1), w_out)
 
 
 def kernel_fits(sizes, tokens, w_b, w_out, taps):

time: 110 us -> 90.5 us (0.82)
  Pallas kernels: 104 us -> 88.5 us
  local copies, waits for them, and re-layouts: 5.28 us -> 1.67 us
    pallas_call x1, Pallas kernels: 104 us -> 88.5 us  [in_one_kernel(): pl.pallas_call(functools.partial(mixer_kernel, sp, tp, halo), out_shape=p...]
    unnamed x2 -> x1, local copies, waits for them, and re-layouts: 5.28 us -> 1.67 us
where the time goes in v2:
time: 90.5 us; the launch traced here: 90.2 us
  Pallas kernels  88.5 us (98%)
  local copies, waits for them, and re-layouts  1.67 us (2%)
    pallas_call x1, Pallas kernels, in_one_kernel(): pl.pallas_call(functools.partial(mixer_kernel, sp, tp, halo), out_shape=p...  88.5 us

profile of v2, /device:TPU:0, one launch (start us, length us, event | category | flops | bytes accessed | tf_op | source)
XLA Modules:
  0.0 90.2 jit_solution(12455798406144631011)
XLA Ops:
  0.0 88.5 %shard_map.82 = bf16[768,2048]{1,0:T(8,128)(2,1)S(1)} custom-call(bf16[768,2048]{1,0:T(8,128)(2,1)} %tok.1, f32[2,2048]{1,0:T(2,128)} %gain_pre.1, f32[2,2048]{1,0:T(2,128)} %gain_post.1, bf16[2,512,128]{2,1,0:T(8,128)(2,1)} %w_b.1, bf16[2,512,128]{2,1,0:T(8,128)(2,1)} %w_c.1, bf16[2,512,128]{2,1,0:T(8,128)(2,1)} %w_x.1, f32[3,2,512]{2,1,0:T(2,128)} %bitcast.1, ...), custom_call_target="tpu_custom_call" | custom-call | tf_op jit(solution)/shard_map/pallas_call | solution.py:485
  88.5 1.7 %copy.10 = bf16[768,2048]{1,0:T(8,128)(2,1)} copy(bf16[768,2048]{1,0:T(8,128)(2,1)S(1)} %shard_map.82) | data formatting | bytes 6291456
